TPU v7x, 32 devices: a whole 2x2x4 slice. The times are simulated.
32 devices in a mesh: ep: 8 (over z, x), tp: 4 (over y, core).
Axes of the slice: x: 2, y: 2, z: 4, core: 2. Of those that a mesh axis runs over, the one named last changes fastest.
Arguments:
- queries: bfloat16 [1024, 4096], P('ep', 'tp'), may hold values from -112 to 112
- key_rows: bfloat16 [1024, 4096], P('ep', 'tp'), may hold values from -8.1 to 8.1
- values: bfloat16 [1024, 4096], P('ep', 'tp'), may hold values from -6 to 6
- lambdas: float32 [16], P('tp'), may hold values from 0.3 to 0.8
- head_gain: float32 [256], replicated, may hold values from 0.1 to 1.9
- tokens: bfloat16 [512, 4096], P('ep'), may hold values from -6 to 6
- moe_gain: float32 [4096], replicated, may hold values from 0.1 to 1.9
- routes: int32 [512, 2], P('ep'), may hold values from 0 to 7, all different within a row; in each aligned block of 64 rows (0 to 63, 64 to 127, ...) at most 32 rows name the same one
- route_scores: float32 [512, 2], P('ep'), may hold values from -6 to 6
- w_gate: bfloat16 [8, 4096, 2048], P('ep', None, 'tp'), may hold values from -0.09375 to 0.09375
- w_up: bfloat16 [8, 4096, 2048], P('ep', None, 'tp'), may hold values from -0.09375 to 0.09375
- w_down: bfloat16 [8, 2048, 4096], P('ep', 'tp'), may hold values from -0.125 to 0.125
Outputs:
- attended: bfloat16 [1024, 4096], P('ep', 'tp')
- expert_out: bfloat16 [512, 4096], P('ep', 'tp')
Inputs may be any that keep to these rules, and one draw needn't show every extreme that they name: `routes`: each row names 2 different experts. Among the rows of one index of ep at most 32 name the same expert, and some index reaches 32 in every draw.
All inputs are finite; a program needn't handle non-finite values.
Results may differ from a plain program's by a relative error of at most 0.018.
Values may be sent and summed in bfloat16 or wider, within the bound.
A program may use at most 64 MiB of HBM per device.

v0:
```python
import jax
import jax.numpy as jnp
from jax import lax
from jax.sharding import PartitionSpec as P

QKD = 128
VD = 256
TOP = 2
neg_big = -1e30
head_eps = 1e-05
moe_eps = 1e-06
head_scale = 0.8


def slot_table(routes, experts, capacity):
    flat_routes = routes.reshape(-1)
    onehot = (flat_routes[:, None] == jnp.arange(experts, dtype=jnp.int32)[None, :]).astype(
        jnp.int32
    )
    before = jnp.cumsum(onehot, axis=0) - onehot
    position = jnp.sum(before * onehot, axis=1)
    return (flat_routes * capacity + position).reshape(routes.shape)


def fold_block(state, query_group, query_pos, key_heads, value_heads, key_pos):
    maxima, denominators, accumulated = state
    scores = jnp.einsum(
        "qhmd,khmd->hmqk", query_group, key_heads, preferred_element_type=jnp.float32
    ) * QKD ** (-0.5)
    visible = key_pos[None, :] <= query_pos[:, None]
    scores = jnp.where(visible, scores, neg_big)
    new_max = jnp.maximum(maxima, jnp.max(scores, axis=-1))
    weights = jnp.where(visible, jnp.exp(scores - new_max[..., None]), 0.0)
    accumulated = jnp.einsum(
        "hmqk,khd->hmqd", weights, value_heads, precision=lax.Precision.HIGHEST
    )
    denominators = jnp.sum(weights, axis=-1)
    return (new_max, denominators, accumulated)


def local(
    queries,
    key_rows,
    values,
    lambdas,
    head_gain,
    tokens,
    moe_gain,
    routes,
    route_scores,
    w_gate,
    w_up,
    w_down,
):
    rows_a = queries.shape[0]
    half_rows = rows_a // 2
    head_local = lambdas.shape[0]
    ep_count = lax.axis_size("ep")
    ep_index = lax.axis_index("ep")
    early_queries = queries[:half_rows]
    later_queries = queries[half_rows:]
    early_pos = ep_index * rows_a + jnp.arange(half_rows, dtype=jnp.int32)
    later_pos = ep_index * rows_a + half_rows + jnp.arange(half_rows, dtype=jnp.int32)
    query_groups = (
        early_queries.reshape(half_rows, head_local, 2, QKD),
        later_queries.reshape(half_rows, head_local, 2, QKD),
    )
    position_groups = (early_pos, later_pos)
    start_state = (
        jnp.full((head_local, 2, half_rows), neg_big, jnp.float32),
        jnp.zeros((head_local, 2, half_rows), jnp.float32),
        jnp.zeros((head_local, 2, half_rows, VD), jnp.float32),
    )
    totals = (start_state, start_state)
    row_start = jnp.int32(0)
    key_block = lax.all_gather(key_rows, "ep", axis=0, tiled=True)
    value_block = lax.all_gather(values, "ep", axis=0, tiled=True)
    key_count = key_block.shape[0]
    key_heads = key_block.reshape(key_count, head_local, 2, QKD)
    value_heads = value_block.reshape(key_count, head_local, VD).astype(jnp.float32)
    key_pos = jnp.arange(key_count, dtype=jnp.int32)
    updated = []
    for attend_group_index in range(2):
        state = totals[attend_group_index]
        query_group = query_groups[attend_group_index]
        query_pos = position_groups[attend_group_index]
        state = lax.cond(
            row_start <= query_pos[-1],
            lambda held: fold_block(held, query_group, query_pos, key_heads, value_heads, key_pos),
            lambda held: held,
            state,
        )
        updated.append(state)
    folded = (updated[0], updated[1])
    attended_groups = []
    for group_index in range(2):
        maxima, denominators, accumulated = folded[group_index]
        mixed_out = (
            accumulated[:, 0] / denominators[:, 0, :, None]
            - lambdas[:, None, None] * accumulated[:, 1] / denominators[:, 1, :, None]
        )
        scaled = mixed_out * lax.rsqrt(
            jnp.mean(mixed_out * mixed_out, axis=-1, keepdims=True) + head_eps
        )
        scaled = scaled * head_gain * head_scale
        attended_groups.append(
            scaled.transpose(1, 0, 2).reshape(half_rows, head_local * VD).astype(jnp.bfloat16)
        )
    later_out = attended_groups[1]
    attended = jnp.concatenate([attended_groups[0], later_out], axis=0)
    rows_b = tokens.shape[0]
    capacity = 2 * TOP * rows_b // ep_count
    token_f32 = tokens.astype(jnp.float32)
    normed = (
        token_f32
        * lax.rsqrt(jnp.mean(token_f32 * token_f32, axis=-1, keepdims=True) + moe_eps)
        * moe_gain
    ).astype(jnp.bfloat16)
    gate_weights = jax.nn.softmax(route_scores, axis=-1)
    slot_of = slot_table(routes, ep_count, capacity)
    row_ids = jnp.broadcast_to(jnp.arange(rows_b, dtype=jnp.int32)[:, None], slot_of.shape)
    row_of_slot = (
        jnp.zeros((ep_count * capacity,), jnp.int32)
        .at[slot_of.reshape(-1)]
        .set(row_ids.reshape(-1))
    )
    gate_local = w_gate[0]
    up_local = w_up[0]
    down_local = w_down[0]
    outgoing = normed[row_of_slot]
    arrived = lax.all_to_all(outgoing, "ep", split_axis=0, concat_axis=0, tiled=True)
    gate_act = jnp.dot(arrived, gate_local, preferred_element_type=jnp.float32)
    up_act = jnp.dot(arrived, up_local, preferred_element_type=jnp.float32)
    hidden = (jax.nn.silu(gate_act) * up_act).astype(jnp.bfloat16)
    summed = lax.psum_scatter(
        lax.dot_general(
            down_local, hidden, (((0,), (1,)), ((), ())), preferred_element_type=jnp.float32
        ).astype(jnp.bfloat16),
        "tp",
        scatter_dimension=0,
        tiled=True,
    )
    returned = lax.all_to_all(summed, "ep", split_axis=1, concat_axis=1, tiled=True)
    slot_ids = jnp.arange(ep_count * capacity, dtype=jnp.int32)
    combined = jnp.zeros((rows_b, returned.shape[0]), jnp.float32)
    for choice_index in range(TOP):
        picker = (slot_of[:, choice_index, None] == slot_ids[None, :]).astype(jnp.bfloat16)
        picked = lax.dot_general(
            picker, returned, (((1,), (1,)), ((), ())), preferred_element_type=jnp.float32
        )
        combined = combined + gate_weights[:, choice_index, None] * picked
    expert_out = combined.astype(jnp.bfloat16)
    return (attended, expert_out)


def solution(mesh):
    return jax.shard_map(
        local,
        mesh=mesh,
        in_specs=(
            P("ep", "tp"),
            P("ep", "tp"),
            P("ep", "tp"),
            P("tp"),
            P(),
            P("ep", None),
            P(),
            P("ep", None),
            P("ep", None),
            P("ep", None, "tp"),
            P("ep", None, "tp"),
            P("ep", "tp", None),
        ),
        out_specs=(P("ep", "tp"), P("ep", "tp")),
        check_vma=False,
    )
```

profile of v0, /device:TPU:0, one launch (start us, length us, event | category | flops | bytes accessed | tf_op | source)
XLA Modules:
  0.0 190.7 jit_solution(13893074613434656306)
XLA Ops:
  8.1 1.9 copy.24
  9.9 0.8 copy.34
  11.8 1.0 scatter_custom_fusion
  12.8 1.2 fusion.42
  14.0 0.9 fusion.44
  15.0 3.2 %gather_fusion = bf16[256,4096]{1,0:T(8,128)(2,1)} fusion(bf16[64,4096]{1,0:T(8,128)(2,1)S(1)} %fusion.44, s32[1024]{0:T(1024)S(1)} %pad_clamp_fusion), kind=kCustom, calls=%fused_computation | custom fusion | bytes 4195328 | tf_op jit(solution)/shard_map/gather | solution.py:130
  18.2 7.4 %all-to-all-start = ((bf16[8,32,4096]{2,1,0:T(8,128)(2,1)}), bf16[8,32,4096]{2,1,0:T(8,128)(2,1)S(1)}, u32[]{:S(2)}, u32[]{:S(2)}) async-start(bf16[8,32,4096]{2,1,0:T(8,128)(2,1)} %bitcast.20), calls=%async_computation | async-start | bytes 4194304 | tf_op jit(solution)/shard_map/all_to_all | solution.py:131
  25.6 0.8 copy.23
  26.5 69.8 %all-to-all-done = bf16[8,32,4096]{2,1,0:T(8,128)(2,1)S(1)} async-done(((bf16[8,32,4096]{2,1,0:T(8,128)(2,1)}), bf16[8,32,4096]{2,1,0:T(8,128)(2,1)S(1)}, u32[]{:S(2)}, u32[]{:S(2)}) %all-to-all-start) | async-done | bytes 2097184 | tf_op jit(solution)/shard_map/all_to_all | solution.py:131
  96.3 3.5 %fusion.32 = f32[256,512]{1,0:T(8,128)S(1)} fusion(bf16[256,4096]{1,0:T(8,128)(2,1)S(1)} %bitcast.99, bf16[1,4096,512]{2,1,0:T(8,128)(2,1)} %param.25), kind=kOutput, calls=%fused_computation.43 | convolution fusion | flops 1073741824 | bytes 6815744 | tf_op jit(solution)/shard_map/dot_general | solution.py:132
  99.8 7.4 %fusion.28 = bf16[4096,256]{0,1:T(8,128)(2,1)} fusion(bf16[1,512,4096]{2,1,0:T(8,128)(2,1)} %param.27, bf16[256,4096]{1,0:T(8,128)(2,1)S(1)} %bitcast.100, bf16[1,4096,512]{2,1,0:T(8,128)(2,1)} %param.26, f32[256,512]{1,0:T(8,128)S(1)} %fusion.32), kind=kOutput, calls=%fused_computation.39 | convolution fusion | flops 2149318656 | bytes 13107200 | tf_op jit(solution)/shard_map/dot_general | solution.py:136
  110.0 4.1 %convert.3 = f32[1024,4,256]{0,2,1:T(8,128)} convert(bf16[1024,4,256]{0,2,1:T(8,128)(2,1)} %bitcast.98) | non-fusion elementwise | flops 1048576 | bytes 6291456 | tf_op jit(solution)/shard_map/convert_element_type | solution.py:80
  114.1 33.2 %all-gather.3.cloned.1.call-done = bf16[1024,1024]{0,1:T(8,128)(2,1)} async-done(((bf16[128,1024]{0,1:T(8,128)(2,1)}), bf16[1024,1024]{0,1:T(8,128)(2,1)}) %all-gather.3.cloned.1.call-update) | async-done | bytes 2097168 | tf_op jit(solution)/shard_map/all_gather | solution.py:76
  147.3 8.6 %conditional.3 = (f32[4,2,64]{2,1,0:T(2,128)S(1)}, f32[4,2,64,256]{3,2,1,0:T(8,128)S(1)}) conditional(s32[]{:T(128)} %bitcast.10, () %tuple.26, (s32[1024]{0:T(1024)S(1)}, s32[64]{0:T(128)S(1)}, bf16[128,1024]{1,0:T(8,128)(2,1)S(1)}, bf16[1024,4,2,128]{0,3,2,1:T(8,128)(2,1)}, f32[1024,4,256]{0,2,1:T(8,128)}) %tuple.56), branch_computations={%region_5.6_spmd, %region_6.9_spmd} | conditional | flops 1751186944 | bytes 30818604 | solution.py:87
  147.5 2.4 %fusion.16 = (f32[4,2,64]{2,1,0:T(2,128)S(1)}, f32[4,2,64,1024]{3,2,1,0:T(8,128)S(1)}) fusion(pred[64,1024]{1,0:T(8,128)(4,1)S(1)} %broadcast_compare_fusion.1, bf16[1024,4,2,128]{0,3,2,1:T(8,128)(2,1)} %get-tuple-element.52, bf16[64,4,2,128]{3,2,1,0:T(2,128)(2,1)S(1)} %reshape.109), kind=kOutput, calls=%fused_computation.24 | convolution fusion | flops 135790080 | bytes 4392960 | tf_op jit(solution)/shard_map/cond/branch_1_fun/qhmd,khmd->hmqk/dot_general | solution.py:27
  150.3 4.8 %fusion.14 = f32[4,2,64,256]{3,2,1,0:T(8,128)S(1)} fusion(f32[1024,4,256]{0,2,1:T(8,128)S(1)} %copy-done, f32[4,2,64,1024]{3,2,1,0:T(8,128)S(1)} %get-tuple-element.63, f32[4,2,64]{2,1,0:T(2,128)S(1)} %broadcast_maximum_fusion.1, pred[64,1024]{1,0:T(8,128)(4,1)S(1)} %broadcast_compare_fusion.1), kind=kOutput, calls=%fused_computation.20 | convolution fusion | flops 1612709888 | bytes 6883328 | tf_op jit(solution)/shard_map/cond/branch_1_fun/hmqk,khd->hmqd/dot_general | solution.py:34
  155.2 0.7 fusion.17
  155.9 8.8 %conditional.2 = (f32[4,2,64]{2,1,0:T(2,128)S(1)}, f32[4,2,64,256]{3,2,1,0:T(8,128)S(1)}) conditional(s32[]{:T(128)} %bitcast.2, () %tuple.24, (s32[1024]{0:T(1024)S(1)}, s32[64]{0:T(128)S(1)}, bf16[128,1024]{1,0:T(8,128)(2,1)S(1)}, bf16[1024,4,2,128]{0,3,2,1:T(8,128)(2,1)}, f32[1024,4,256]{0,2,1:T(8,128)}) %tuple.57), branch_computations={%region_0.0_spmd, %region_1.4_spmd} | conditional | flops 1751186944 | bytes 30818604 | solution.py:87
  156.3 2.4 %fusion.2 = (f32[4,2,64]{2,1,0:T(2,128)S(1)}, f32[4,2,64,1024]{3,2,1,0:T(8,128)S(1)}) fusion(pred[64,1024]{1,0:T(8,128)(4,1)S(1)} %broadcast_compare_fusion, bf16[1024,4,2,128]{0,3,2,1:T(8,128)(2,1)} %get-tuple-element.47, bf16[64,4,2,128]{3,2,1,0:T(2,128)(2,1)S(1)} %reshape.108), kind=kOutput, calls=%fused_computation.6 | convolution fusion | flops 135790080 | bytes 4392960 | tf_op jit(solution)/shard_map/cond/branch_1_fun/qhmd,khmd->hmqk/dot_general | solution.py:27
  159.1 4.8 %fusion = f32[4,2,64,256]{3,2,1,0:T(8,128)S(1)} fusion(f32[1024,4,256]{0,2,1:T(8,128)S(1)} %copy-done.1, f32[4,2,64,1024]{3,2,1,0:T(8,128)S(1)} %get-tuple-element.61, f32[4,2,64]{2,1,0:T(2,128)S(1)} %broadcast_maximum_fusion, pred[64,1024]{1,0:T(8,128)(4,1)S(1)} %broadcast_compare_fusion), kind=kOutput, calls=%fused_computation.2 | convolution fusion | flops 1612709888 | bytes 6883328 | tf_op jit(solution)/shard_map/cond/branch_1_fun/hmqk,khd->hmqd/dot_general | solution.py:34
  164.7 3.5 %all-to-all-start.1 = ((bf16[1024,8,32]{0,2,1:T(8,128)(2,1)}), bf16[1024,8,32]{0,2,1:T(8,128)(2,1)S(1)}, u32[]{:S(2)}, u32[]{:S(2)}) async-start(bf16[1024,8,32]{0,2,1:T(8,128)(2,1)} %bitcast.101), calls=%async_computation.2 | async-start | bytes 1048576 | tf_op jit(solution)/shard_map/all_to_all | solution.py:143
  168.8 0.7 pad_maximum_fusion
  169.5 12.6 %all-to-all-done.1 = bf16[1024,8,32]{0,2,1:T(8,128)(2,1)S(1)} async-done(((bf16[1024,8,32]{0,2,1:T(8,128)(2,1)}), bf16[1024,8,32]{0,2,1:T(8,128)(2,1)S(1)}, u32[]{:S(2)}, u32[]{:S(2)}) %all-to-all-start.1) | async-done | bytes 524320 | tf_op jit(solution)/shard_map/all_to_all | solution.py:143
  182.4 0.9 fusion.41
  (65 shorter events, 5.3 us)
Async XLA Ops:
  8.0 6.0 %copy-start.2 = (bf16[64,4096]{1,0:T(8,128)(2,1)S(1)}, bf16[64,4096]{1,0:T(8,128)(2,1)}, u32[]{:S(2)}) copy-start(bf16[64,4096]{1,0:T(8,128)(2,1)} %param.21) | copy-start | bytes 1572868
  8.0 102.0 %all-gather.5.cloned.1.call-start = ((), (), s32[]{:S(2)}) async-start(), calls=%async_computation.4 | async-start | bytes 2359296 | tf_op jit(solution)/shard_map/all_gather | solution.py:77
  18.2 7.5 %copy-start.3 = (bf16[128,1024]{1,0:T(8,128)(2,1)S(1)}, bf16[128,1024]{1,0:T(8,128)(2,1)}, u32[]{:S(2)}) copy-start(bf16[128,1024]{1,0:T(8,128)(2,1)} %param.17) | copy-start | bytes 786436
  18.2 78.2 %all-to-all-start = ((bf16[8,32,4096]{2,1,0:T(8,128)(2,1)}), bf16[8,32,4096]{2,1,0:T(8,128)(2,1)S(1)}, u32[]{:S(2)}, u32[]{:S(2)}) async-start(bf16[8,32,4096]{2,1,0:T(8,128)(2,1)} %bitcast.20), calls=%async_computation | async-start | bytes 4194304 | tf_op jit(solution)/shard_map/all_to_all | solution.py:131
  25.6 121.7 %all-gather.3.cloned.1.call-start = ((), (), s32[]{:S(2)}) async-start(), calls=%async_computation.3 | async-start | bytes 2359296 | tf_op jit(solution)/shard_map/all_gather | solution.py:76
  26.5 138.2 %reduce-scatter.2.cloned.1.call-start = ((), (), s32[]{:S(2)}) async-start(), calls=%async_computation.5 | async-start | bytes 2621440 | tf_op jit(solution)/shard_map/reduce_scatter | solution.py:135
  107.2 2.5 %copy-start.5 = (f32[64,2]{0,1:T(2,128)S(1)}, f32[64,2]{0,1:T(2,128)}, u32[]{:S(2)}) copy-start(f32[64,2]{0,1:T(2,128)} %param.24) | copy-start | bytes 1540
  110.0 37.3 %copy-start.4 = (bf16[128,1024]{1,0:T(8,128)(2,1)S(1)}, bf16[128,1024]{1,0:T(8,128)(2,1)}, u32[]{:S(2)}) copy-start(bf16[128,1024]{1,0:T(8,128)(2,1)} %param.16) | copy-start | bytes 786436
  147.5 2.8 %copy-start = (f32[1024,4,256]{0,2,1:T(8,128)S(1)}, f32[1024,4,256]{0,2,1:T(8,128)}, u32[]{:S(2)}) copy-start(f32[1024,4,256]{0,2,1:T(8,128)} %get-tuple-element.53) | copy-start | bytes 12582916 | tf_op jit(solution)/shard_map/cond
  155.9 12.4 %copy-start.7 = (f32[4]{0:T(128)S(1)}, f32[4]{0:T(128)}, u32[]{:S(2)}) copy-start(f32[4]{0:T(128)} %param.19) | copy-start | bytes 52
  156.3 2.8 %copy-start.1 = (f32[1024,4,256]{0,2,1:T(8,128)S(1)}, f32[1024,4,256]{0,2,1:T(8,128)}, u32[]{:S(2)}) copy-start(f32[1024,4,256]{0,2,1:T(8,128)} %get-tuple-element.48) | copy-start | bytes 12582916 | tf_op jit(solution)/shard_map/cond
  164.7 4.0 %copy-start.6 = (f32[256]{0:T(256)S(1)}, f32[256]{0:T(256)}, u32[]{:S(2)}) copy-start(f32[256]{0:T(256)} %param.20) | copy-start | bytes 3076
  164.7 17.4 %all-to-all-start.1 = ((bf16[1024,8,32]{0,2,1:T(8,128)(2,1)}), bf16[1024,8,32]{0,2,1:T(8,128)(2,1)S(1)}, u32[]{:S(2)}, u32[]{:S(2)}) async-start(bf16[1024,8,32]{0,2,1:T(8,128)(2,1)} %bitcast.101), calls=%async_computation.2 | async-start | bytes 1048576 | tf_op jit(solution)/shard_map/all_to_all | solution.py:143
Sparse Core Ops, SparseCore 0:
  10.9 83.9 all-gather.4
  97.5 49.7 all-gather.2
Sparse Core Ops, SparseCore 1:
  107.3 30.1 reduce-scatter.1
where the time goes:
time: 191 us
  waiting for transfers between devices  116 us (61%)
  matrix products  26.5 us (14%)
  between operations  17.1 us (9%)
  starting transfers between devices  11 us (6%)
  local copies, waits for them, and re-layouts  10.5 us (5%)
  other arithmetic  9.63 us (5%)
    all_to_all x1, waiting for transfers between devices, local(): lax.all_to_all(outgoing, 'ep', split_axis=0, concat_axis=0, tiled=True)  69.8 us
    all_gather x1, waiting for transfers between devices, local(): key_block = lax.all_gather(key_rows, 'ep', axis=0, tiled=True)  33.2 us
    all_to_all x1, waiting for transfers between devices, local(): lax.all_to_all(summed, 'ep', split_axis=1, concat_axis=1, tiled=True)  12.6 us
    dot_general x2, matrix products, fold_block(): jnp.einsum('hmqk,khd->hmqd', weights, value_heads, precision=lax.Precisio...  9.67 us
    all_to_all x1, starting transfers between devices, local(): lax.all_to_all(outgoing, 'ep', split_axis=0, concat_axis=0, tiled=True)  7.41 us
    dot_general x1, matrix products, local(): lax.dot_general(down_local, hidden, (((0,), (1,)), ((), ())), preferred_e...  7.37 us
    dot_general x2, matrix products, fold_block(): jnp.einsum('qhmd,khmd->hmqk', query_group, key_heads, preferred_element_t...  4.85 us
    convert_element_type x1, other arithmetic, local(): value_block.reshape(key_count, head_local, VD).astype(jnp.float32)  4.08 us
  transfers between devices with their start and end apart: 5, of which 3 were waited for; matrix products, arithmetic and copies ran while one was open for 22% of the time, Pallas kernels for 0%

commit v1 on v0

--- a/solution.py
+++ b/solution.py
@@ -1,3 +1,4 @@
+import functools
 import jax
 import jax.numpy as jnp
 from jax import lax
@@ -10,6 +11,30 @@
 head_eps = 1e-05
 moe_eps = 1e-06
 head_scale = 0.8
+
+
+def view_the_circles(vector, along_axis):
+    value_now = lax.axis_size(along_axis)
+    state_now = lax.axis_index(along_axis)
+    new, oldest = (value_now, state_now)
+    arr_out = vector.shape[1] // new
+    raw_out = list(vector.shape)
+    raw_out[1] = arr_out
+    x_next = raw_out[1]
+    raw_out[1] = x_next * new
+    y = jnp.zeros(raw_out, vector.dtype)
+    j0 = 0
+    while j0 < new:
+        val2 = lax.dynamic_slice_in_dim(vector, (oldest ^ j0) * arr_out, arr_out, axis=1)
+        if j0:
+            z2 = tuple(((j, j ^ j0) for j in range(new)))
+            val2 = lax.ppermute(val2, along_axis, z2)
+        y = lax.dynamic_update_slice_in_dim(y, val2, (oldest ^ j0) * x_next, axis=1)
+        j0 = j0 + 1
+    return y
+
+
+balance_squares_now = functools.partial(view_the_circles, along_axis="ep")
 
 
 def slot_table(routes, experts, capacity):
@@ -140,7 +165,7 @@
         scatter_dimension=0,
         tiled=True,
     )
-    returned = lax.all_to_all(summed, "ep", split_axis=1, concat_axis=1, tiled=True)
+    returned = balance_squares_now(summed)
     slot_ids = jnp.arange(ep_count * capacity, dtype=jnp.int32)
     combined = jnp.zeros((rows_b, returned.shape[0]), jnp.float32)
     for choice_index in range(TOP):

time: 191 us -> 191 us (level)
  waiting for transfers between devices: 116 us -> 108 us
  starting transfers between devices: 11 us -> 18.8 us
    all_to_all x1 -> x0, waiting for transfers between devices: 12.6 us -> none  [local(): lax.all_to_all(summed, 'ep', split_axis=1, concat_axis=1, tiled=True)]
    ppermute x0 -> x7, starting transfers between devices: none -> 11.3 us  [view_the_circles(): val2 = lax.ppermute(val2, along_axis, z2)]
    ppermute x0 -> x7, waiting for transfers between devices: none -> 4.63 us  [view_the_circles(): val2 = lax.ppermute(val2, along_axis, z2)]
    all_to_all x1 -> x0, starting transfers between devices: 3.5 us -> none  [local(): lax.all_to_all(summed, 'ep', split_axis=1, concat_axis=1, tiled=True)]
  transfers between devices with their start and end apart: 5 -> 11, of which waited for: 3 -> 4; matrix products, arithmetic and copies ran while one was open for 22% -> 23% of each run, Pallas kernels for 0% -> 0%
where the time goes in v1:
time: 191 us
  waiting for transfers between devices  108 us (57%)
  matrix products  26.5 us (14%)
  starting transfers between devices  18.8 us (10%)
  between operations  17.2 us (9%)
  local copies, waits for them, and re-layouts  11.1 us (6%)
  other arithmetic  9.65 us (5%)
    all_to_all x1, waiting for transfers between devices, local(): lax.all_to_all(outgoing, 'ep', split_axis=0, concat_axis=0, tiled=True)  69.8 us
    all_gather x1, waiting for transfers between devices, local(): key_block = lax.all_gather(key_rows, 'ep', axis=0, tiled=True)  33 us
    ppermute x7, starting transfers between devices, view_the_circles(): val2 = lax.ppermute(val2, along_axis, z2)  11.3 us
    dot_general x2, matrix products, fold_block(): jnp.einsum('hmqk,khd->hmqd', weights, value_heads, precision=lax.Precisio...  9.66 us
    all_to_all x1, starting transfers between devices, local(): lax.all_to_all(outgoing, 'ep', split_axis=0, concat_axis=0, tiled=True)  7.41 us
    dot_general x1, matrix products, local(): lax.dot_general(down_local, hidden, (((0,), (1,)), ((), ())), preferred_e...  7.31 us
    dot_general x2, matrix products, fold_block(): jnp.einsum('qhmd,khmd->hmqk', query_group, key_heads, preferred_element_t...  4.84 us
    ppermute x7, waiting for transfers between devices, view_the_circles(): val2 = lax.ppermute(val2, along_axis, z2)  4.63 us
  transfers between devices with their start and end apart: 11, of which 4 were waited for; matrix products, arithmetic and copies ran while one was open for 23% of the time, Pallas kernels for 0%

profile of v1, /device:TPU:0, one launch (start us, length us, event | category | flops | bytes accessed | tf_op | source)
XLA Modules:
  0.0 190.8 jit_solution(11887304590745487940)
XLA Ops:
  8.1 1.8 copy.24
  11.7 1.0 scatter_custom_fusion
  12.7 1.2 fusion.42
  14.9 3.2 %gather_fusion = bf16[256,4096]{1,0:T(8,128)(2,1)} fusion(bf16[64,4096]{1,0:T(8,128)(2,1)S(1)} %fusion.44, s32[1024]{0:T(1024)S(1)} %pad_clamp_fusion), kind=kCustom, calls=%fused_computation | custom fusion | bytes 4195328 | tf_op jit(solution)/shard_map/gather | solution.py:155
  18.1 7.4 %all-to-all-start = ((bf16[8,32,4096]{2,1,0:T(8,128)(2,1)}), bf16[8,32,4096]{2,1,0:T(8,128)(2,1)S(1)}, u32[]{:S(2)}, u32[]{:S(2)}) async-start(bf16[8,32,4096]{2,1,0:T(8,128)(2,1)} %bitcast.20), calls=%async_computation | async-start | bytes 4194304 | tf_op jit(solution)/shard_map/all_to_all | solution.py:156
  26.5 69.8 %all-to-all-done = bf16[8,32,4096]{2,1,0:T(8,128)(2,1)S(1)} async-done(((bf16[8,32,4096]{2,1,0:T(8,128)(2,1)}), bf16[8,32,4096]{2,1,0:T(8,128)(2,1)S(1)}, u32[]{:S(2)}, u32[]{:S(2)}) %all-to-all-start) | async-done | bytes 2097184 | tf_op jit(solution)/shard_map/all_to_all | solution.py:156
  96.3 3.5 %fusion.32 = f32[256,512]{1,0:T(8,128)S(1)} fusion(bf16[256,4096]{1,0:T(8,128)(2,1)S(1)} %bitcast.95, bf16[1,4096,512]{2,1,0:T(8,128)(2,1)} %param.25), kind=kOutput, calls=%fused_computation.43 | convolution fusion | flops 1073741824 | bytes 6815744 | tf_op jit(solution)/shard_map/dot_general | solution.py:157
  99.8 7.3 %fusion.28 = bf16[4096,256]{0,1:T(8,128)(2,1)} fusion(bf16[1,512,4096]{2,1,0:T(8,128)(2,1)} %param.27, bf16[256,4096]{1,0:T(8,128)(2,1)S(1)} %bitcast.96, bf16[1,4096,512]{2,1,0:T(8,128)(2,1)} %param.26, f32[256,512]{1,0:T(8,128)S(1)} %fusion.32), kind=kOutput, calls=%fused_computation.39 | convolution fusion | flops 2149318656 | bytes 13107200 | tf_op jit(solution)/shard_map/dot_general | solution.py:161
  110.0 4.1 %convert.3 = f32[1024,4,256]{0,2,1:T(8,128)} convert(bf16[1024,4,256]{0,2,1:T(8,128)(2,1)} %bitcast.94) | non-fusion elementwise | flops 1048576 | bytes 6291456 | tf_op jit(solution)/shard_map/convert_element_type | solution.py:105
  114.1 33.0 %all-gather.3.cloned.1.call-done = bf16[1024,1024]{0,1:T(8,128)(2,1)} async-done(((bf16[128,1024]{0,1:T(8,128)(2,1)}), bf16[1024,1024]{0,1:T(8,128)(2,1)}) %all-gather.3.cloned.1.call-update) | async-done | bytes 2097168 | tf_op jit(solution)/shard_map/all_gather | solution.py:101
  147.2 8.2 %conditional.2 = (f32[4,2,64]{2,1,0:T(2,128)S(1)}, f32[4,2,64,256]{3,2,1,0:T(8,128)S(1)}) conditional(s32[]{:T(128)} %bitcast.2, () %tuple.24, (s32[1024]{0:T(1024)S(1)}, s32[64]{0:T(128)S(1)}, bf16[128,1024]{1,0:T(8,128)(2,1)S(1)}, bf16[1024,4,2,128]{0,3,2,1:T(8,128)(2,1)}, f32[1024,4,256]{0,2,1:T(8,128)}) %tuple.63), branch_computations={%region_0.0_spmd, %region_1.4_spmd} | conditional | flops 1751186944 | bytes 30818604 | solution.py:112
  147.4 2.4 %fusion.2 = (f32[4,2,64]{2,1,0:T(2,128)S(1)}, f32[4,2,64,1024]{3,2,1,0:T(8,128)S(1)}) fusion(pred[64,1024]{1,0:T(8,128)(4,1)S(1)} %broadcast_compare_fusion, bf16[1024,4,2,128]{0,3,2,1:T(8,128)(2,1)} %get-tuple-element.47, bf16[64,4,2,128]{3,2,1,0:T(2,128)(2,1)S(1)} %reshape.106), kind=kOutput, calls=%fused_computation.6 | convolution fusion | flops 135790080 | bytes 4392960 | tf_op jit(solution)/shard_map/cond/branch_1_fun/qhmd,khmd->hmqk/dot_general | solution.py:52
  150.5 4.8 %fusion = f32[4,2,64,256]{3,2,1,0:T(8,128)S(1)} fusion(f32[1024,4,256]{0,2,1:T(8,128)S(1)} %copy-done, f32[4,2,64,1024]{3,2,1,0:T(8,128)S(1)} %get-tuple-element.61, f32[4,2,64]{2,1,0:T(2,128)S(1)} %broadcast_maximum_fusion, pred[64,1024]{1,0:T(8,128)(4,1)S(1)} %broadcast_compare_fusion), kind=kOutput, calls=%fused_computation.2 | convolution fusion | flops 1612709888 | bytes 6883328 | tf_op jit(solution)/shard_map/cond/branch_1_fun/hmqk,khd->hmqd/dot_general | solution.py:59
  155.4 8.2 %conditional.3 = (f32[4,2,64]{2,1,0:T(2,128)S(1)}, f32[4,2,64,256]{3,2,1,0:T(8,128)S(1)}) conditional(s32[]{:T(128)} %bitcast.10, () %tuple.26, (s32[1024]{0:T(1024)S(1)}, s32[64]{0:T(128)S(1)}, bf16[128,1024]{1,0:T(8,128)(2,1)S(1)}, bf16[1024,4,2,128]{0,3,2,1:T(8,128)(2,1)}, f32[1024,4,256]{0,2,1:T(8,128)}) %tuple.64), branch_computations={%region_5.6_spmd, %region_6.9_spmd} | conditional | flops 1751186944 | bytes 30818604 | solution.py:112
  155.6 2.4 %fusion.16 = (f32[4,2,64]{2,1,0:T(2,128)S(1)}, f32[4,2,64,1024]{3,2,1,0:T(8,128)S(1)}) fusion(pred[64,1024]{1,0:T(8,128)(4,1)S(1)} %broadcast_compare_fusion.1, bf16[1024,4,2,128]{0,3,2,1:T(8,128)(2,1)} %get-tuple-element.52, bf16[64,4,2,128]{3,2,1,0:T(2,128)(2,1)S(1)} %reshape.107), kind=kOutput, calls=%fused_computation.24 | convolution fusion | flops 135790080 | bytes 4392960 | tf_op jit(solution)/shard_map/cond/branch_1_fun/qhmd,khmd->hmqk/dot_general | solution.py:52
  158.8 4.8 %fusion.14 = f32[4,2,64,256]{3,2,1,0:T(8,128)S(1)} fusion(f32[1024,4,256]{0,2,1:T(8,128)S(1)} %copy-done.1, f32[4,2,64,1024]{3,2,1,0:T(8,128)S(1)} %get-tuple-element.63, f32[4,2,64]{2,1,0:T(2,128)S(1)} %broadcast_maximum_fusion.1, pred[64,1024]{1,0:T(8,128)(4,1)S(1)} %broadcast_compare_fusion.1), kind=kOutput, calls=%fused_computation.20 | convolution fusion | flops 1612709888 | bytes 6883328 | tf_op jit(solution)/shard_map/cond/branch_1_fun/hmqk,khd->hmqd/dot_general | solution.py:59
  164.3 1.1 constant_dynamic-slice_fusion
  165.5 1.5 collective-permute-start
  167.7 2.0 %collective-permute-start.2 = (bf16[1024,32]{0,1:T(8,128)(2,1)S(1)}, bf16[1024,32]{0,1:T(8,128)(2,1)S(1)}, u32[]{:S(2)}, u32[]{:S(2)}) collective-permute-start(bf16[1024,32]{0,1:T(8,128)(2,1)S(1)} %get-tuple-element.68), channel_id=1, source_target_pairs={{0,12},{4,8},{8,4},{12,0},{16,28},{20,24},{24,20},{28,16},{1,13},{... | collective-permute-start | bytes 196616 | tf_op jit(solution)/shard_map/ppermute | solution.py:31
  169.7 1.5 collective-permute-start.3
  171.2 2.3 %collective-permute-start.4 = (bf16[1024,32]{0,1:T(8,128)(2,1)S(1)}, bf16[1024,32]{0,1:T(8,128)(2,1)S(1)}, u32[]{:S(2)}, u32[]{:S(2)}) collective-permute-start(bf16[1024,32]{0,1:T(8,128)(2,1)S(1)} %get-tuple-element.66), channel_id=1, source_target_pairs={{0,20},{4,16},{8,28},{12,24},{16,4},{20,0},{24,12},{28,8},{1,21},{... | collective-permute-start | bytes 196616 | tf_op jit(solution)/shard_map/ppermute | solution.py:31
  174.1 3.3 %collective-permute-start.6 = (bf16[1024,32]{0,1:T(8,128)(2,1)S(1)}, bf16[1024,32]{0,1:T(8,128)(2,1)S(1)}, u32[]{:S(2)}, u32[]{:S(2)}) collective-permute-start(bf16[1024,32]{0,1:T(8,128)(2,1)S(1)} %get-tuple-element.64), channel_id=1, source_target_pairs={{0,28},{4,24},{8,20},{12,16},{16,12},{20,8},{24,4},{28,0},{1,29},{... | collective-permute-start | bytes 196616 | tf_op jit(solution)/shard_map/ppermute | solution.py:31
  177.5 1.4 collective-permute-done.3
  178.9 3.3 %collective-permute-done.4 = bf16[1024,32]{0,1:T(8,128)(2,1)S(1)} collective-permute-done((bf16[1024,32]{0,1:T(8,128)(2,1)S(1)}, bf16[1024,32]{0,1:T(8,128)(2,1)S(1)}, u32[]{:S(2)}, u32[]{:S(2)}) %collective-permute-start.4) | collective-permute-done | bytes 65568 | tf_op jit(solution)/shard_map/ppermute | solution.py:31
  (86 shorter events, 10.1 us)
Async XLA Ops:
  8.0 6.0 %copy-start.2 = (bf16[64,4096]{1,0:T(8,128)(2,1)S(1)}, bf16[64,4096]{1,0:T(8,128)(2,1)}, u32[]{:S(2)}) copy-start(bf16[64,4096]{1,0:T(8,128)(2,1)} %param.21) | copy-start | bytes 1572868
  8.0 102.0 %all-gather.5.cloned.1.call-start = ((), (), s32[]{:S(2)}) async-start(), calls=%async_computation.3 | async-start | bytes 2359296 | tf_op jit(solution)/shard_map/all_gather | solution.py:102
  18.1 7.5 %copy-start.3 = (bf16[128,1024]{1,0:T(8,128)(2,1)S(1)}, bf16[128,1024]{1,0:T(8,128)(2,1)}, u32[]{:S(2)}) copy-start(bf16[128,1024]{1,0:T(8,128)(2,1)} %param.17) | copy-start | bytes 786436
  18.1 78.2 %all-to-all-start = ((bf16[8,32,4096]{2,1,0:T(8,128)(2,1)}), bf16[8,32,4096]{2,1,0:T(8,128)(2,1)S(1)}, u32[]{:S(2)}, u32[]{:S(2)}) async-start(bf16[8,32,4096]{2,1,0:T(8,128)(2,1)} %bitcast.20), calls=%async_computation | async-start | bytes 4194304 | tf_op jit(solution)/shard_map/all_to_all | solution.py:156
  25.5 121.6 %all-gather.3.cloned.1.call-start = ((), (), s32[]{:S(2)}) async-start(), calls=%async_computation.2 | async-start | bytes 2359296 | tf_op jit(solution)/shard_map/all_gather | solution.py:101
  26.5 137.8 %reduce-scatter.2.cloned.1.call-start = ((), (), s32[]{:S(2)}) async-start(), calls=%async_computation.4 | async-start | bytes 2621440 | tf_op jit(solution)/shard_map/reduce_scatter | solution.py:160
  107.1 2.6 %copy-start.5 = (f32[64,2]{0,1:T(2,128)S(1)}, f32[64,2]{0,1:T(2,128)}, u32[]{:S(2)}) copy-start(f32[64,2]{0,1:T(2,128)} %param.24) | copy-start | bytes 1540
  110.0 37.2 %copy-start.4 = (bf16[128,1024]{1,0:T(8,128)(2,1)S(1)}, bf16[128,1024]{1,0:T(8,128)(2,1)}, u32[]{:S(2)}) copy-start(bf16[128,1024]{1,0:T(8,128)(2,1)} %param.16) | copy-start | bytes 786436
  147.4 3.2 %copy-start = (f32[1024,4,256]{0,2,1:T(8,128)S(1)}, f32[1024,4,256]{0,2,1:T(8,128)}, u32[]{:S(2)}) copy-start(f32[1024,4,256]{0,2,1:T(8,128)} %get-tuple-element.48) | copy-start | bytes 12582916 | tf_op jit(solution)/shard_map/cond
  155.4 8.3 %copy-start.7 = (f32[4]{0:T(128)S(1)}, f32[4]{0:T(128)}, u32[]{:S(2)}) copy-start(f32[4]{0:T(128)} %param.19) | copy-start | bytes 52
  155.4 8.6 %copy-start.6 = (f32[256]{0:T(256)S(1)}, f32[256]{0:T(256)}, u32[]{:S(2)}) copy-start(f32[256]{0:T(256)} %param.20) | copy-start | bytes 3076
  155.6 3.2 %copy-start.1 = (f32[1024,4,256]{0,2,1:T(8,128)S(1)}, f32[1024,4,256]{0,2,1:T(8,128)}, u32[]{:S(2)}) copy-start(f32[1024,4,256]{0,2,1:T(8,128)} %get-tuple-element.53) | copy-start | bytes 12582916 | tf_op jit(solution)/shard_map/cond
  165.5 8.1 %collective-permute-start = (bf16[1024,32]{0,1:T(8,128)(2,1)S(1)}, bf16[1024,32]{0,1:T(8,128)(2,1)S(1)}, u32[]{:S(2)}, u32[]{:S(2)}) collective-permute-start(bf16[1024,32]{0,1:T(8,128)(2,1)S(1)} %get-tuple-element.70), channel_id=1, source_target_pairs={{0,4},{4,0},{8,12},{12,8},{16,20},{20,16},{24,28},{28,24},{1,5},{5... | collective-permute-start | bytes 196616 | tf_op jit(solution)/shard_map/ppermute | solution.py:31
  167.7 6.4 %collective-permute-start.1 = (bf16[1024,32]{0,1:T(8,128)(2,1)S(1)}, bf16[1024,32]{0,1:T(8,128)(2,1)S(1)}, u32[]{:S(2)}, u32[]{:S(2)}) collective-permute-start(bf16[1024,32]{0,1:T(8,128)(2,1)S(1)} %get-tuple-element.69), channel_id=1, source_target_pairs={{0,8},{4,12},{8,0},{12,4},{16,24},{20,28},{24,16},{28,20},{1,9},{5... | collective-permute-start | bytes 196616 | tf_op jit(solution)/shard_map/ppermute | solution.py:31
  167.7 9.8 %collective-permute-start.2 = (bf16[1024,32]{0,1:T(8,128)(2,1)S(1)}, bf16[1024,32]{0,1:T(8,128)(2,1)S(1)}, u32[]{:S(2)}, u32[]{:S(2)}) collective-permute-start(bf16[1024,32]{0,1:T(8,128)(2,1)S(1)} %get-tuple-element.68), channel_id=1, source_target_pairs={{0,12},{4,8},{8,4},{12,0},{16,28},{20,24},{24,20},{28,16},{1,13},{... | collective-permute-start | bytes 196616 | tf_op jit(solution)/shard_map/ppermute | solution.py:31
  169.7 9.1 %collective-permute-start.3 = (bf16[1024,32]{0,1:T(8,128)(2,1)S(1)}, bf16[1024,32]{0,1:T(8,128)(2,1)S(1)}, u32[]{:S(2)}, u32[]{:S(2)}) collective-permute-start(bf16[1024,32]{0,1:T(8,128)(2,1)S(1)} %get-tuple-element.67), channel_id=1, source_target_pairs={{0,16},{4,20},{8,24},{12,28},{16,0},{20,4},{24,8},{28,12},{1,17},{... | collective-permute-start | bytes 196616 | tf_op jit(solution)/shard_map/ppermute | solution.py:31
  171.2 10.9 %collective-permute-start.4 = (bf16[1024,32]{0,1:T(8,128)(2,1)S(1)}, bf16[1024,32]{0,1:T(8,128)(2,1)S(1)}, u32[]{:S(2)}, u32[]{:S(2)}) collective-permute-start(bf16[1024,32]{0,1:T(8,128)(2,1)S(1)} %get-tuple-element.66), channel_id=1, source_target_pairs={{0,20},{4,16},{8,28},{12,24},{16,4},{20,0},{24,12},{28,8},{1,21},{... | collective-permute-start | bytes 196616 | tf_op jit(solution)/shard_map/ppermute | solution.py:31
  173.6 8.6 %collective-permute-start.5 = (bf16[1024,32]{0,1:T(8,128)(2,1)S(1)}, bf16[1024,32]{0,1:T(8,128)(2,1)S(1)}, u32[]{:S(2)}, u32[]{:S(2)}) collective-permute-start(bf16[1024,32]{0,1:T(8,128)(2,1)S(1)} %get-tuple-element.65), channel_id=1, source_target_pairs={{0,24},{4,28},{8,16},{12,20},{16,8},{20,12},{24,0},{28,4},{1,25},{... | collective-permute-start | bytes 196616 | tf_op jit(solution)/shard_map/ppermute | solution.py:31
  174.1 8.1 %collective-permute-start.6 = (bf16[1024,32]{0,1:T(8,128)(2,1)S(1)}, bf16[1024,32]{0,1:T(8,128)(2,1)S(1)}, u32[]{:S(2)}, u32[]{:S(2)}) collective-permute-start(bf16[1024,32]{0,1:T(8,128)(2,1)S(1)} %get-tuple-element.64), channel_id=1, source_target_pairs={{0,28},{4,24},{8,20},{12,16},{16,12},{20,8},{24,4},{28,0},{1,29},{... | collective-permute-start | bytes 196616 | tf_op jit(solution)/shard_map/ppermute | solution.py:31
Sparse Core Ops, SparseCore 0:
  10.9 83.9 all-gather.4
  97.4 49.6 all-gather.2
Sparse Core Ops, SparseCore 1:
  107.2 30.1 reduce-scatter.1
